TPU v7x, 32 devices: a whole 2x2x4 slice. The times are simulated.
32 devices in a mesh: dp: 4 (over y, x), kv: 4 (over z), tp: 2 (over core).
Axes of the slice: x: 2, y: 2, z: 4, core: 2. Of those that a mesh axis runs over, the one named last changes fastest.
Arguments:
- piece_tokens: bfloat16 [256, 2048], P(('dp', 'kv')), parts along dimension 0, may hold values from -6 to 6
- dec_tokens: bfloat16 [192, 4, 2048], P(('dp', 'kv')), parts along dimension 0, may hold values from -6 to 6
- norm_gain: float32 [2048], replicated, may hold values from 0.1 to 1.9
- query_weight: bfloat16 [2048, 1024], P(None, 'tp'), may hold values from -0.375 to 0.375
- key_weight: bfloat16 [2048, 256], P(None, 'tp'), may hold values from -0.125 to 0.125
- value_weight: bfloat16 [2048, 256], P(None, 'tp'), may hold values from -0.125 to 0.125
- gate_weight: bfloat16 [2048, 8], P(None, 'tp'), may hold values from -0.125 to 0.125
- gate_bias: float32 [8], P('tp'), may hold values from 3.4 to 11
- out_weight: bfloat16 [1024, 2048], P('tp'), may hold values from -0.1875 to 0.1875
- out_gain: float32 [2048], replicated, may hold values from 0.1 to 1.9
- past_keys: bfloat16 [4096, 2, 128], P(('dp', 'kv'), 'tp'), parts along dimension 0, may hold values from -41 to 41
- past_values: bfloat16 [4096, 2, 128], P(('dp', 'kv'), 'tp'), parts along dimension 0, may hold values from -6 to 6
- past_gate: float32 [8, 4096], P('tp', ('dp', 'kv')), parts along dimension 1, may hold values from -1024 to 0
- dec_keys: bfloat16 [192, 512, 2, 128], P(('dp', 'kv'), None, 'tp'), parts along dimension 0, may hold values from -41 to 41
- dec_values: bfloat16 [192, 512, 2, 128], P(('dp', 'kv'), None, 'tp'), parts along dimension 0, may hold values from -6 to 6
- dec_gate: float32 [192, 8, 512], P(('dp', 'kv'), 'tp'), parts along dimension 0, may hold values from -512 to 0
- dec_lengths: int32 [192], P(('dp', 'kv')), parts along dimension 0, may hold values from 1 to 512, as said below
Outputs:
- piece_out: bfloat16 [256, 2048], P(('dp', 'kv')), parts along dimension 0
- dec_out: bfloat16 [192, 4, 2048], P(('dp', 'kv')), parts along dimension 0
There are 4 independent parts, one for each index of `dp`. A program takes and returns all parts, laid end to end along the dimension named above; an argument that names none is the same for every part. Nothing has to cross between parts.
Inputs may be any that keep to these rules, and one draw needn't show every extreme that they name: `dec_lengths`: some decoding sequence has all 512 slots live in every draw.
All inputs are finite; a program needn't handle non-finite values.
Results may differ from a plain program's by a relative error of at most 0.015.
Values may be sent and summed in bfloat16 or wider, within the bound.
A program may use at most 64 MiB of HBM per device.

v0:
```python
import jax
import jax.numpy as jnp
from jax import lax
from jax.sharding import PartitionSpec as P

EPS = 1e-06


def rms_scale(source, scale_gain):
    widened = source.astype(jnp.float32)
    return (
        widened * lax.rsqrt(jnp.mean(widened * widened, axis=-1, keepdims=True) + EPS) * scale_gain
    )


def body(
    piece_tokens,
    dec_tokens,
    norm_gain,
    query_weight,
    key_weight,
    value_weight,
    gate_weight,
    gate_bias,
    out_weight,
    out_gain,
    past_keys,
    past_values,
    past_gate,
    dec_keys,
    dec_values,
    dec_gate,
    dec_lengths,
):
    piece_rows = piece_tokens.shape[0]
    model_width = piece_tokens.shape[1]
    kv_local = past_keys.shape[1]
    head_dim = past_keys.shape[2]
    heads_local = gate_bias.shape[0]
    group_size = heads_local // kv_local
    score_scale = head_dim ** (-0.5)
    seq_count = dec_tokens.shape[0]
    new_count = dec_tokens.shape[1]
    kv_count = lax.axis_size("kv")
    position = lax.axis_index("kv")
    all_rows = jnp.concatenate(
        [piece_tokens, dec_tokens.reshape(seq_count * new_count, model_width)], axis=0
    )
    normed = rms_scale(all_rows, norm_gain).astype(jnp.bfloat16)
    queries = jnp.dot(normed, query_weight, preferred_element_type=jnp.float32).astype(jnp.bfloat16)
    key_rows = jnp.dot(normed, key_weight, preferred_element_type=jnp.float32).astype(jnp.bfloat16)
    value_rows = jnp.dot(normed, value_weight, preferred_element_type=jnp.float32).astype(
        jnp.bfloat16
    )
    log_gates = jax.nn.log_sigmoid(
        jnp.dot(normed, gate_weight, preferred_element_type=jnp.float32) + gate_bias
    )
    piece_queries = queries[:piece_rows]
    piece_keys = key_rows[:piece_rows].reshape(piece_rows, kv_local, head_dim)
    piece_values = value_rows[:piece_rows].reshape(piece_rows, kv_local, head_dim)
    local_run = jnp.cumsum(log_gates[:piece_rows], axis=0)
    gathered_run = lax.all_gather(local_run, "kv", axis=0, tiled=True)
    shard_run = gathered_run.reshape(kv_count, piece_rows, heads_local)
    totals = shard_run[:, -1]
    before = jnp.cumsum(totals, axis=0) - totals
    piece_run = (shard_run + before[:, None, :]).reshape(kv_count * piece_rows, heads_local)
    own_run = lax.dynamic_slice_in_dim(piece_run, position * piece_rows, piece_rows, 0)
    key_place = position * piece_rows + jnp.arange(piece_rows)
    gate_groups = jnp.moveaxis(past_gate.reshape(kv_local, group_size, -1), 1, 0)
    own_groups = jnp.moveaxis(own_run.reshape(piece_rows, kv_local, group_size), 2, 0)
    shard_queries = lax.all_gather(piece_queries, "kv", axis=0, tiled=True)
    row_count = shard_queries.shape[0]
    query_groups = jnp.moveaxis(
        shard_queries.reshape(row_count, kv_local, group_size, head_dim), 2, 0
    )
    run_groups = jnp.moveaxis(piece_run.reshape(row_count, kv_local, group_size), 2, 0)
    row_place = jnp.arange(row_count)
    causal = key_place[None, :] <= row_place[:, None]

    def one_group(inputs):
        query_one, run_one, gate_one, key_run_one = inputs
        row_bias = run_one.T[:, :, None]
        past_scores = (
            jnp.einsum("nkd,pkd->knp", query_one, past_keys, preferred_element_type=jnp.float32)
            * score_scale
        )
        past_scores = past_scores + gate_one[:, None, :] + row_bias
        new_scores = (
            jnp.einsum("nkd,jkd->knj", query_one, piece_keys, preferred_element_type=jnp.float32)
            * score_scale
        )
        new_scores = new_scores + row_bias - key_run_one.T[:, None, :]
        new_scores = jnp.where(causal[None], new_scores, -jnp.inf)
        row_top = jnp.maximum(jnp.max(past_scores, axis=-1), jnp.max(new_scores, axis=-1))
        past_exp = jnp.exp(past_scores - row_top[..., None])
        new_exp = jnp.exp(new_scores - row_top[..., None])
        row_total = jnp.sum(past_exp, axis=-1) + jnp.sum(new_exp, axis=-1)
        summed = jnp.einsum(
            "knp,pkd->nkd",
            past_exp.astype(jnp.bfloat16),
            past_values,
            preferred_element_type=jnp.float32,
        )
        summed = summed + jnp.einsum(
            "knj,jkd->nkd",
            new_exp.astype(jnp.bfloat16),
            piece_values,
            preferred_element_type=jnp.float32,
        )
        return (summed, row_top.T, row_total.T)

    group_out, group_top, group_total = lax.map(
        one_group, (query_groups, run_groups, gate_groups, own_groups)
    )
    group_out = jnp.moveaxis(group_out, 0, 2).reshape(row_count, heads_local, head_dim)
    group_top = jnp.moveaxis(group_top, 0, 2).reshape(row_count, heads_local)
    group_total = jnp.moveaxis(group_total, 0, 2).reshape(row_count, heads_local)
    arrived = (
        lax.all_to_all(
            group_out.reshape(kv_count, piece_rows, heads_local, head_dim),
            "kv",
            split_axis=0,
            concat_axis=0,
            tiled=True,
        ),
        lax.all_to_all(
            group_top.reshape(kv_count, piece_rows, heads_local),
            "kv",
            split_axis=0,
            concat_axis=0,
            tiled=True,
        ),
        lax.all_to_all(
            group_total.reshape(kv_count, piece_rows, heads_local),
            "kv",
            split_axis=0,
            concat_axis=0,
            tiled=True,
        ),
    )
    global_top = jnp.max(arrived[1], axis=0)
    weights = jnp.exp(arrived[1] - global_top)
    row_total = jnp.sum(arrived[2] * weights, axis=0)
    piece_result = jnp.sum(arrived[0] * weights[..., None], axis=0) / row_total[..., None]
    piece_attention = piece_result.reshape(piece_rows, heads_local * head_dim).astype(jnp.bfloat16)
    dec_queries = queries[piece_rows:].reshape(seq_count, new_count, kv_local, group_size, head_dim)
    dec_new_keys = key_rows[piece_rows:].reshape(seq_count, new_count, kv_local, head_dim)
    dec_new_values = value_rows[piece_rows:].reshape(seq_count, new_count, kv_local, head_dim)
    dec_run = jnp.cumsum(log_gates[piece_rows:].reshape(seq_count, new_count, heads_local), axis=1)
    past_len = dec_keys.shape[1]
    slot_index = jnp.arange(past_len)
    last_gate = jnp.sum(
        jnp.where(slot_index[None, None, :] == (dec_lengths - 1)[:, None, None], dec_gate, 0.0),
        axis=2,
    )
    query_bias = jnp.moveaxis(dec_run.reshape(seq_count, new_count, kv_local, group_size), 1, 3)
    past_bias = last_gate.reshape(seq_count, kv_local, group_size)[..., None, None]
    dec_gate_groups = dec_gate.reshape(seq_count, kv_local, group_size, past_len)
    new_scores = (
        jnp.einsum(
            "stkgd,sukd->skgtu", dec_queries, dec_new_keys, preferred_element_type=jnp.float32
        )
        * score_scale
    )
    new_scores = new_scores + query_bias[..., None] - query_bias[..., None, :]
    new_causal = jnp.arange(new_count)[None, :] <= jnp.arange(new_count)[:, None]
    new_scores = jnp.where(new_causal, new_scores, -jnp.inf)
    new_top = jnp.max(new_scores, axis=-1)
    new_exp = jnp.exp(new_scores - new_top[..., None])
    start_dec = (
        jnp.einsum(
            "skgtu,sukd->skgtd",
            new_exp.astype(jnp.bfloat16),
            dec_new_values,
            preferred_element_type=jnp.float32,
        ),
        new_top,
        jnp.sum(new_exp, axis=-1),
    )
    block_scores = (
        jnp.einsum("stkgd,spkd->skgtp", dec_queries, dec_keys, preferred_element_type=jnp.float32)
        * score_scale
    )
    block_scores = (
        block_scores + query_bias[..., None] + past_bias - dec_gate_groups[:, :, :, None, :]
    )
    live_mask = jnp.arange(past_len)[None, :] < dec_lengths[:, None]
    block_scores = jnp.where(live_mask[:, None, None, None, :], block_scores, -jnp.inf)
    row_top = jnp.maximum(start_dec[1], jnp.max(block_scores, axis=-1))
    block_exp = jnp.exp(block_scores - row_top[..., None])
    rescale = jnp.exp(start_dec[1] - row_top)
    summed = start_dec[0] * rescale[..., None] + jnp.einsum(
        "skgtp,spkd->skgtd",
        block_exp.astype(jnp.bfloat16),
        dec_values,
        preferred_element_type=jnp.float32,
    )
    dec_attention = summed / (start_dec[2] * rescale + jnp.sum(block_exp, axis=-1))[..., None]
    dec_attention = (
        jnp.transpose(dec_attention, (0, 3, 1, 2, 4))
        .reshape(seq_count * new_count, heads_local * head_dim)
        .astype(jnp.bfloat16)
    )
    attention = jnp.concatenate([piece_attention, dec_attention], axis=0)
    partial_rows = jnp.dot(attention, out_weight, preferred_element_type=jnp.float32)
    mixed = lax.psum(partial_rows.astype(jnp.bfloat16), "tp").astype(jnp.float32)
    final_rows = rms_scale(mixed, out_gain).astype(jnp.bfloat16)
    return (
        final_rows[:piece_rows],
        final_rows[piece_rows:].reshape(seq_count, new_count, model_width),
    )


def solution(mesh):
    return jax.shard_map(
        body,
        mesh=mesh,
        in_specs=(
            P(("dp", "kv"), None),
            P(("dp", "kv"), None, None),
            P(),
            P(None, "tp"),
            P(None, "tp"),
            P(None, "tp"),
            P(None, "tp"),
            P("tp"),
            P("tp", None),
            P(),
            P(("dp", "kv"), "tp", None),
            P(("dp", "kv"), "tp", None),
            P("tp", ("dp", "kv")),
            P(("dp", "kv"), None, "tp", None),
            P(("dp", "kv"), None, "tp", None),
            P(("dp", "kv"), "tp", None),
            P(("dp", "kv")),
        ),
        out_specs=(P(("dp", "kv"), None), P(("dp", "kv"), None, None)),
        check_vma=False,
    )
```

profile of v0, /device:TPU:0, one launch (start us, length us, event | category | flops | bytes accessed | tf_op | source)
XLA Modules:
  0.0 105.0 jit_solution(5508176570152350641)
XLA Ops:
  7.2 1.1 %reshape.318 = bf16[48,2048]{1,0:T(8,128)(2,1)S(1)} reshape(bf16[12,4,2048]{2,1,0:T(4,128)(2,1)} %param.20) | data formatting | bytes 393216 | tf_op jit(solution)/shard_map/reshape | solution.py:47
  8.4 1.0 fusion.69
  9.4 1.1 %fusion.87 = f32[64,4]{0,1:T(4,128)S(1)} fusion(bf16[2048,4]{0,1:T(4,128)(2,1)} %param.25, f32[4]{0:T(128)} %param.26, f32[2048]{0:T(1024)} %param.21, f32[64]{0:T(128)S(1)} %add_rsqrt_fusion.1, bf16[48,2048]{1,0:T(8,128)(2,1)S(1)} %reshape.318, bf16[16,2048]{1,0:T(8,128)(2,1)} %param.19), kind=kOutput, calls=%fused_computation.106 | convolution fusion | flops 1968384 | bytes 288016 | tf_op jit(solution)/shard_map/dot_general | solution.py:56
  10.7 13.6 %all-gather = f32[4,16,4]{1,2,0:T(4,128)S(1)} all-gather(f32[1,16,4]{1,2,0:T(4,128)S(1)} %bitcast.224), channel_id=1, replica_groups=mesh['dp'=4,'kv'=4,'tp'=2] {'kv'}, dimensions={0}, use_global_device_ids=true | all-gather | bytes 1280 | tf_op jit(solution)/shard_map/all_gather | solution.py:62
  24.8 0.9 transpose_reshape.3
  25.6 1.4 %convolution_convert_fusion.3 = bf16[64,128]{1,0:T(8,128)(2,1)S(1)} fusion(bf16[2048,128]{1,0:T(8,128)(2,1)} %param.23, f32[2048]{0:T(1024)} %param.21, f32[64]{0:T(128)S(1)} %add_rsqrt_fusion.1, bf16[48,2048]{1,0:T(8,128)(2,1)S(1)} %reshape.318, bf16[16,2048]{1,0:T(8,128)(2,1)} %param.19), kind=kOutput, calls=%fused_computation.61 | convolution fusion | flops 34480128 | bytes 811264 | tf_op jit(solution)/shard_map/dot_general | solution.py:51
  27.1 0.3 convolution_convert_fusion.2
  27.4 0.5 convolution_convert_fusion.1
  27.9 13.1 %all_gather.6 = bf16[64,512]{1,0:T(8,128)(2,1)S(1)} all-gather(bf16[16,512]{1,0:T(8,128)(2,1)S(1)} %slice.44), channel_id=1, replica_groups=mesh['dp'=4,'kv'=4,'tp'=2] {'kv'}, dimensions={0}, use_global_device_ids=true | all-gather | bytes 81920 | tf_op jit(solution)/shard_map/all_gather | solution.py:71
  41.2 4.4 %while.15 = (s32[]{:T(128)}, f32[4,64,1,128]{3,1,2,0:T(8,128)S(1)}, f32[4,64,1]{1,2,0:T(1,128)S(1)}, f32[4,64,1]{1,2,0:T(1,128)S(1)}, bf16[4,64,1,128]{3,1,2,0:T...) while((s32[]{:T(128)}, f32[4,64,1,128]{3,1,2,0:T(8,128)S(1)}, ...), condition=%wide.region_8.9_spmd.clone, body=%wide.region_3.8_spmd.clone.sunk | while | flops 9062274 | bytes 495149 | solution.py:112
  41.4 0.3 fusion.126
  42.5 0.3 fusion.126
  45.7 0.6 copy.73
  46.3 3.4 %all-to-all-start.1 = ((f32[4,16,4]{1,2,0:T(4,128)}), f32[4,16,4]{1,2,0:T(4,128)S(1)}, u32[]{:S(2)}, u32[]{:S(2)}) async-start(f32[4,16,4]{1,2,0:T(4,128)} %copy.73), calls=%async_computation.1 | async-start | bytes 16384 | tf_op jit(solution)/shard_map/all_to_all | solution.py:126
  50.1 0.6 reduce_window_sum.38
  50.9 0.6 fusion.95
  51.6 0.4 copy.80
  52.1 2.0 %fusion.96 = (f32[12,4,4]{1,2,0:T(4,128)S(1)}, f32[12,1,4,4,512]{4,2,3,0,1:T(4,128)S(1)}) fusion(f32[12,4,512]{2,1,0:T(4,128)S(1)} %copy-done.5, f32[12,4]{1,0:T(8,128)S(1)} %select_reduce_fusion, f32[12,4,4]{1,2,0:T(4,128)S(1)} %copy.78, bf16[12,4,4,128]{3,2,1,0:T(4,128)(2,1)S(1)} %reshape.325, bf16[12,512,1,128]{3,1,2,0:T(8,128)(2,1)} %param.32, ...), kind=kOutput, calls=%fused_computation.119 | convolution fusion | flops 25755456 | bytes 2121408 | tf_op jit(solution)/shard_map/stkgd,spkd->skgtp/dot_general | solution.py:181
  54.2 0.3 fusion.77
  54.9 0.6 copy.75
  55.7 5.1 %all-to-all-start.2 = ((f32[4,16,4]{1,2,0:T(4,128)}), f32[4,16,4]{1,2,0:T(4,128)S(1)}, u32[]{:S(2)}, u32[]{:S(2)}) async-start(f32[4,16,4]{1,2,0:T(4,128)} %copy.75), calls=%async_computation.2 | async-start | bytes 16384 | tf_op jit(solution)/shard_map/all_to_all | solution.py:133
  60.8 1.8 %fusion.65 = bf16[12,4,1,4,128]{4,1,3,0,2:T(4,128)(2,1)S(1)} fusion(f32[12,4,4,128]{3,2,1,0:T(4,128)S(1)} %convolution_multiply_fusion.2, bf16[12,512,1,128]{3,1,2,0:T(8,128)(2,1)} %param.33, bf16[12,4,4,512]{3,1,2,0:T(4,128)(2,1)S(1)} %get-tuple-element.191, f32[12,4,4]{2,1,0:T(4,128)S(1)} %copy.84), kind=kOutput, calls=%fused_computation.59 | convolution fusion | flops 25239552 | bytes 1917696 | tf_op jit(solution)/shard_map/skgtp,spkd->skgtd/dot_general | solution.py:192
  62.6 0.7 copy.72
  63.3 3.2 %all-to-all-done.2 = f32[4,16,4]{1,2,0:T(4,128)S(1)} async-done(((f32[4,16,4]{1,2,0:T(4,128)}), f32[4,16,4]{1,2,0:T(4,128)S(1)}, u32[]{:S(2)}, u32[]{:S(2)}) %all-to-all-start.2) | async-done | bytes 1056 | tf_op jit(solution)/shard_map/all_to_all | solution.py:133
  66.5 3.3 %all-to-all-start = ((f32[4,16,4,128]{3,1,2,0:T(8,128)}), f32[4,16,4,128]{3,1,2,0:T(8,128)S(1)}, u32[]{:S(2)}, u32[]{:S(2)}) async-start(f32[4,16,4,128]{3,1,2,0:T(8,128)} %copy.72), calls=%async_computation | async-start | bytes 262144 | tf_op jit(solution)/shard_map/all_to_all | solution.py:119
  69.9 5.8 %all-to-all-done = f32[4,16,4,128]{3,1,2,0:T(8,128)S(1)} async-done(((f32[4,16,4,128]{3,1,2,0:T(8,128)}), f32[4,16,4,128]{3,1,2,0:T(8,128)S(1)}, u32[]{:S(2)}, u32[]{:S(2)}) %all-to-all-start) | async-done | bytes 131104 | tf_op jit(solution)/shard_map/all_to_all | solution.py:119
  75.9 1.2 %convolution_convert_fusion = bf16[64,2048]{1,0:T(8,128)(2,1)} fusion(bf16[512,2048]{1,0:T(8,128)(2,1)S(1)} %copy-done, bf16[48,512]{1,0:T(8,128)(2,1)S(1)} %bitcast.214, bf16[16,512]{1,0:T(8,128)(2,1)S(1)} %copy_bitcast_fusion.2), kind=kOutput, calls=%fused_computation.38 | convolution fusion | flops 134479872 | bytes 2424832 | tf_op jit(solution)/shard_map/dot_general | solution.py:205
  77.1 17.4 %all-reduce.2.cloned.1.call-done = bf16[64,2048]{1,0:T(8,128)(2,1)} async-done(((bf16[64,2048]{1,0:T(8,128)(2,1)}), bf16[64,2048]{1,0:T(8,128)(2,1)}) %all-reduce.2.cloned.1.call-update) | async-done | bytes 262160 | tf_op jit(solution)/shard_map/psum | solution.py:206
  94.6 1.1 %fusion.72 = f32[64]{0:T(128)S(1)} fusion(bf16[64,2048]{1,0:T(8,128)(2,1)} %all-reduce.2.cloned.1.call-done), kind=kLoop, calls=%fused_computation.72 | loop fusion | flops 393152 | bytes 262400 | tf_op jit(solution)/shard_map/reduce_sum | solution.py:12
  95.7 1.1 %fusion.74 = bf16[64,2048]{1,0:T(8,128)(2,1)S(1)} fusion(bf16[64,2048]{1,0:T(8,128)(2,1)} %all-reduce.2.cloned.1.call-done, f32[2048]{0:T(1024)S(1)} %copy-done.8, f32[64]{0:T(128)S(1)} %add_rsqrt_fusion), kind=kLoop, calls=%fused_computation.74 | loop fusion | flops 524288 | bytes 532736 | tf_op jit(solution)/shard_map/convert_element_type | solution.py:207
  96.8 0.6 slice.51
  97.4 0.8 reshape.331
  (116 shorter events, 6.2 us)
Async XLA Ops:
  7.2 68.7 %copy-start = (bf16[512,2048]{1,0:T(8,128)(2,1)S(1)}, bf16[512,2048]{1,0:T(8,128)(2,1)}, u32[]{:S(2)}) copy-start(bf16[512,2048]{1,0:T(8,128)(2,1)} %param.27) | copy-start | bytes 6291460
  7.2 19.8 %copy-start.4 = (bf16[16,2048]{1,0:T(8,128)(2,1)S(1)}, bf16[16,2048]{1,0:T(8,128)(2,1)}, u32[]{:S(2)}) copy-start(bf16[16,2048]{1,0:T(8,128)(2,1)} %param.19) | copy-start | bytes 196612
  7.2 19.8 %copy-start.7 = (f32[2048]{0:T(1024)S(1)}, f32[2048]{0:T(1024)}, u32[]{:S(2)}) copy-start(f32[2048]{0:T(1024)} %param.21) | copy-start | bytes 24580
  7.2 19.8 %copy-start.10 = (bf16[2048,128]{1,0:T(8,128)(2,1)S(1)}, bf16[2048,128]{1,0:T(8,128)(2,1)}, u32[]{:S(2)}) copy-start(bf16[2048,128]{1,0:T(8,128)(2,1)} %param.24) | copy-start | bytes 1572868
  24.8 2.6 %copy-start.1 = (bf16[2048,512]{1,0:T(8,128)(2,1)S(1)}, bf16[2048,512]{1,0:T(8,128)(2,1)}, u32[]{:S(2)}) copy-start(bf16[2048,512]{1,0:T(8,128)(2,1)} %param.22) | copy-start | bytes 6291460
  27.0 14.2 %copy-start.2 = (bf16[256,1,128]{2,0,1:T(8,128)(2,1)S(1)}, bf16[256,1,128]{2,0,1:T(8,128)(2,1)}, u32[]{:S(2)}) copy-start(bf16[256,1,128]{2,0,1:T(8,128)(2,1)} %param.29) | copy-start | bytes 196612
  27.0 14.2 %copy-start.3 = (bf16[256,1,128]{2,0,1:T(8,128)(2,1)S(1)}, bf16[256,1,128]{2,0,1:T(8,128)(2,1)}, u32[]{:S(2)}) copy-start(bf16[256,1,128]{2,0,1:T(8,128)(2,1)} %param.30) | copy-start | bytes 196612
  27.4 22.5 %copy-start.6 = (bf16[64,128]{1,0:T(8,128)(2,1)}, bf16[64,128]{1,0:T(8,128)(2,1)S(1)}, u32[]{:S(2)}) copy-start(bf16[64,128]{1,0:T(8,128)(2,1)S(1)} %convolution_convert_fusion.2) | copy-start | bytes 49156
  27.9 21.8 %copy-start.9 = (s32[12]{0:T(128)S(1)}, s32[12]{0:T(128)}, u32[]{:S(2)}) copy-start(s32[12]{0:T(128)} %param.35) | copy-start | bytes 148
  41.2 10.8 %copy-start.5 = (f32[12,4,512]{2,1,0:T(4,128)S(1)}, f32[12,4,512]{2,1,0:T(4,128)}, u32[]{:S(2)}) copy-start(f32[12,4,512]{2,1,0:T(4,128)} %param.34) | copy-start | bytes 294916
  46.3 9.4 %all-to-all-start.1 = ((f32[4,16,4]{1,2,0:T(4,128)}), f32[4,16,4]{1,2,0:T(4,128)S(1)}, u32[]{:S(2)}, u32[]{:S(2)}) async-start(f32[4,16,4]{1,2,0:T(4,128)} %copy.73), calls=%async_computation.1 | async-start | bytes 16384 | tf_op jit(solution)/shard_map/all_to_all | solution.py:126
  50.1 4.6 %slice-start = ((bf16[64,128]{1,0:T(8,128)(2,1)}), bf16[48,128]{1,0:T(8,128)(2,1)S(1)}, s32[]{:S(2)}) async-start(bf16[64,128]{1,0:T(8,128)(2,1)} %copy-done.6), calls=%async_computation.4 | async-start | bytes 24576 | tf_op jit(solution)/shard_map/slice | solution.py:148
  55.7 10.8 %all-to-all-start.2 = ((f32[4,16,4]{1,2,0:T(4,128)}), f32[4,16,4]{1,2,0:T(4,128)S(1)}, u32[]{:S(2)}, u32[]{:S(2)}) async-start(f32[4,16,4]{1,2,0:T(4,128)} %copy.75), calls=%async_computation.2 | async-start | bytes 16384 | tf_op jit(solution)/shard_map/all_to_all | solution.py:133
  62.6 33.1 %copy-start.8 = (f32[2048]{0:T(1024)S(1)}, f32[2048]{0:T(1024)}, u32[]{:S(2)}) copy-start(f32[2048]{0:T(1024)} %param.28) | copy-start | bytes 24580
  66.5 9.2 %all-to-all-start = ((f32[4,16,4,128]{3,1,2,0:T(8,128)}), f32[4,16,4,128]{3,1,2,0:T(8,128)S(1)}, u32[]{:S(2)}, u32[]{:S(2)}) async-start(f32[4,16,4,128]{3,1,2,0:T(8,128)} %copy.72), calls=%async_computation | async-start | bytes 262144 | tf_op jit(solution)/shard_map/all_to_all | solution.py:119
  69.8 24.7 %all-reduce.2.cloned.1.call-start = ((), (), s32[]{:S(2)}) async-start(), calls=%async_computation.3 | async-start | bytes 524288 | tf_op jit(solution)/shard_map/psum | solution.py:206
Sparse Core Ops, SparseCore 0:
  77.2 17.2 all-reduce.1
where the time goes:
time: 106 us; the launch traced here: 105 us
  blocking collectives  26.8 us (25%)
  waiting for transfers between devices  26.5 us (25%)
  between operations  14.4 us (14%)
  matrix products  12.2 us (12%)
  starting transfers between devices  11.9 us (11%)
  local copies, waits for them, and re-layouts  7.15 us (7%)
  other arithmetic  6.01 us (6%)
    psum x1, waiting for transfers between devices, body(): lax.psum(partial_rows.astype(jnp.bfloat16), 'tp').astype(jnp.float32)  17.4 us
    all_gather x1, blocking collectives, body(): gathered_run = lax.all_gather(local_run, 'kv', axis=0, tiled=True)  13.6 us
    all_gather x1, blocking collectives, body(): shard_queries = lax.all_gather(piece_queries, 'kv', axis=0, tiled=True)  13.1 us
    all_to_all x1, waiting for transfers between devices, body(): lax.all_to_all(group_out.reshape(kv_count, piece_rows, heads_local, head_...  5.81 us
    all_to_all x1, starting transfers between devices, body(): lax.all_to_all(group_total.reshape(kv_count, piece_rows, heads_local), 'k...  5.09 us
    all_to_all x1, starting transfers between devices, body(): lax.all_to_all(group_top.reshape(kv_count, piece_rows, heads_local), 'kv'...  3.44 us
    all_to_all x1, starting transfers between devices, body(): lax.all_to_all(group_out.reshape(kv_count, piece_rows, heads_local, head_...  3.33 us
    all_to_all x1, waiting for transfers between devices, body(): lax.all_to_all(group_total.reshape(kv_count, piece_rows, heads_local), 'k...  3.19 us
  transfers between devices with their start and end apart: 4, of which 3 were waited for; matrix products, arithmetic and copies ran while one was open for 8% of the time, Pallas kernels for 0%

commit v1 on v0

v1 whole, which is shorter than its diff:
```python
import functools
import math

import jax
import jax.numpy as jnp
from jax import lax
from jax.experimental import pallas as pl
from jax.experimental.pallas import tpu as pltpu
from jax.sharding import PartitionSpec as P

EPS = 1e-06
MESH = pl.DeviceIdType.MESH
F32 = jnp.float32
BF16 = jnp.bfloat16


def dot(a, b):
    return lax.dot_general(a, b, (((1,), (0,)), ((), ())), preferred_element_type=F32)


def dot_t(a, b):
    return lax.dot_general(a, b, (((1,), (1,)), ((), ())), preferred_element_type=F32)


def rms_scale(source, gain):
    return source * lax.rsqrt(jnp.mean(source * source, axis=-1, keepdims=True) + EPS) * gain


def running_sum(rows, period):
    count, lanes = rows.shape
    place = lax.broadcasted_iota(jnp.int32, (count, lanes), 0)
    place = place & (period - 1) if period & (period - 1) == 0 else lax.rem(place, period)
    step = 1
    while step < period:
        shifted = jnp.concatenate([jnp.zeros((step, lanes), F32), rows[: count - step]], axis=0)
        rows = rows + jnp.where(place >= step, shifted, 0.0)
        step *= 2
    return rows


def kernel(
    kv_count,
    tp_count,
    piece_tokens,
    dec_tokens,
    norm_gain,
    query_weight,
    key_weight,
    value_weight,
    gate_weight,
    gate_bias,
    out_weight,
    out_gain,
    past_keys,
    past_values,
    past_gate,
    dec_keys,
    dec_values,
    dec_gate,
    dec_lengths,
    piece_out,
    dec_out,
    v_piece,
    v_dec,
    v_gain,
    v_wq,
    v_wk,
    v_wv,
    v_wg,
    v_bias,
    v_wo,
    v_ogain,
    v_pk,
    v_pv,
    v_pgate,
    v_dk,
    v_dv,
    v_dgate,
    v_len,
    rows_x,
    q_split,
    run_split,
    att_split,
    q_send,
    q_all,
    run_send,
    run_all,
    part_send,
    part_all,
    stat_send,
    stat_all,
    dec_part,
    dec_parts,
    piece_part,
    piece_parts,
    in_sem,
    dk_sem,
    dv_sem,
    q_ssem,
    q_rsem,
    run_ssem,
    run_rsem,
    part_ssem,
    part_rsem,
    stat_ssem,
    stat_rsem,
    tpd_ssem,
    tpd_rsem,
    tpp_ssem,
    tpp_rsem,
):
    R = v_piece.shape[0]
    S, T, D = v_dec.shape
    H = v_bias.shape[1]
    HD = v_pk.shape[1]
    PL = v_pk.shape[0]
    DP = v_dk.shape[1]
    N = S * T
    groups = dk_sem.shape[0]
    G = S // groups
    scale = HD ** (-0.5)
    me = lax.axis_index("kv")
    core = lax.axis_index("tp")

    loads = {}
    pairs = [
        (piece_tokens, v_piece),
        (dec_tokens, v_dec),
        (norm_gain, v_gain),
        (gate_weight, v_wg),
        (gate_bias, v_bias),
        (query_weight, v_wq),
        (key_weight, v_wk),
        (value_weight, v_wv),
        (dec_gate, v_dgate),
        (dec_lengths, v_len),
        (past_gate, v_pgate),
        (past_keys, v_pk),
        (past_values, v_pv),
    ]
    late = [(out_weight, v_wo), (out_gain, v_ogain)]
    count = 0

    def start_load(src, dst):
        nonlocal count
        loads[id(dst)] = pltpu.make_async_copy(src, dst, in_sem.at[count])
        loads[id(dst)].start()
        count += 1

    for src, dst in pairs:
        start_load(src, dst)
    dec_loads = []
    for g in range(groups):
        part = pl.ds(g * G, G)
        ck = pltpu.make_async_copy(dec_keys.at[part], v_dk.at[part], dk_sem.at[g])
        cv = pltpu.make_async_copy(dec_values.at[part], v_dv.at[part], dv_sem.at[g])
        ck.start()
        cv.start()
        dec_loads.append((ck, cv))
    for src, dst in late:
        start_load(src, dst)

    def ready(*refs):
        for ref in refs:
            loads[id(ref)].wait()

    barrier = pltpu.get_barrier_semaphore()
    for i in range(1, kv_count):
        pl.semaphore_signal(
            barrier, inc=1, device_id={"kv": lax.rem(me + i, kv_count)}, device_id_type=MESH
        )
    for i in range(1, tp_count):
        pl.semaphore_signal(
            barrier, inc=1, device_id={"tp": lax.rem(core + i, tp_count)}, device_id_type=MESH
        )

    ready(v_piece, v_dec, v_gain)
    rows_x[:R, :] = v_piece[...].astype(F32)
    for s in range(S):
        rows_x[R + s * T : R + (s + 1) * T, :] = v_dec[s].astype(F32)
    normed = rms_scale(rows_x[...], v_gain[...]).astype(BF16)
    ready(v_wg, v_bias)
    logits = dot_t(normed, v_wg[...]) + v_bias[...]
    log_gates = jnp.minimum(logits, 0.0) - jnp.log1p(jnp.exp(-jnp.abs(logits)))
    log_gates = jnp.concatenate([log_gates, jnp.zeros((R + N, HD - H), F32)], axis=1)
    local_run = running_sum(log_gates[:R], R)
    dec_run = running_sum(log_gates[R:], T)
    run_send[...] = local_run
    ready(v_wq)
    queries = dot(normed, v_wq[...])
    q_send[...] = queries[:R].astype(BF16)
    pl.semaphore_wait(barrier, kv_count - 1 + tp_count - 1)

    def exchange(src_of, dst, ssem, rsem):
        copies = []
        for i in range(1, kv_count):
            peer = lax.rem(me + i, kv_count)
            copy = pltpu.make_async_remote_copy(
                src_ref=src_of(peer),
                dst_ref=dst.at[me],
                send_sem=ssem.at[i - 1],
                recv_sem=rsem.at[i - 1],
                device_id={"kv": peer},
                device_id_type=MESH,
            )
            copy.start()
            copies.append(copy)
        return copies

    q_copies = exchange(lambda peer: q_send, q_all, q_ssem, q_rsem)
    run_copies = exchange(lambda peer: run_send, run_all, run_ssem, run_rsem)
    q_all[me] = queries[:R].astype(BF16)
    run_all[me] = local_run

    for h in range(H):
        q_split[pl.ds(h, N, stride=H), :] = queries[R:, h * HD : (h + 1) * HD]
        run_split[pl.ds(h, N, stride=H), :] = jnp.broadcast_to(dec_run[:, h : h + 1], (N, HD))
    ready(v_wk, v_wv)
    key_rows = dot(normed, v_wk[...]).astype(BF16)
    value_rows = dot(normed, v_wv[...]).astype(BF16)
    pad = -(R + N) % 128
    runs_t = jnp.transpose(
        jnp.concatenate([local_run, dec_run, jnp.zeros((pad, HD), F32)], axis=0)
    )
    local_t = runs_t[:H, :R]
    dec_t = runs_t[:H, R : R + N]

    qd = q_split[...].astype(BF16)
    new_bias = jnp.concatenate([dec_t] * N, axis=0)
    new_scores = dot_t(qd, key_rows[R:]) * scale + run_split[:, :1] - new_bias
    row_at = lax.broadcasted_iota(jnp.int32, (N * H, N), 0)
    col_at = lax.broadcasted_iota(jnp.int32, (N * H, N), 1)
    col_in = col_at & (T - 1) if T & (T - 1) == 0 else lax.rem(col_at, T)
    keep = (row_at >= H * col_at) & (row_at < H * (col_at - col_in + T))
    new_scores = jnp.where(keep, new_scores, -jnp.inf)

    ready(v_dgate, v_len)
    slot = lax.broadcasted_iota(jnp.int32, (H, DP), 1)

    def decode_group(g):
        ck, cv = dec_loads[g]
        lo, hi = g * G * T * H, (g + 1) * G * T * H
        ck.wait()
        biases, scores = [], []
        for s in range(g * G, (g + 1) * G):
            length = v_len[:, s : s + 1]
            gate = v_dgate[s]
            last = jnp.sum(jnp.where(slot == length - 1, gate, 0.0), axis=1, keepdims=True)
            bias = jnp.where(slot < length, last - gate, -jnp.inf)
            biases.append(jnp.concatenate([bias] * T, axis=0))
            scores.append(dot_t(qd[s * T * H : (s + 1) * T * H], v_dk[s]))
        old = jnp.concatenate(scores, axis=0) * scale + run_split[lo:hi, :1]
        old = old + jnp.concatenate(biases, axis=0)
        new = new_scores[lo:hi]
        top = jnp.maximum(
            jnp.max(old, axis=1, keepdims=True), jnp.max(new, axis=1, keepdims=True)
        )
        old = jnp.exp(old - top)
        new = jnp.exp(new - top)
        total = jnp.sum(old, axis=1, keepdims=True) + jnp.sum(new, axis=1, keepdims=True)
        old = old.astype(BF16)
        cv.wait()
        summed = jnp.concatenate(
            [
                dot(old[i * T * H : (i + 1) * T * H], v_dv[g * G + i])
                for i in range(G)
            ],
            axis=0,
        )
        summed = summed + dot(new.astype(BF16), value_rows[R:])
        att_split[lo:hi, :] = summed / total

    early = max(groups - 1, 1)
    for g in range(early):
        decode_group(g)

    ready(v_pgate, v_pk, v_pv)
    for copy in run_copies:
        copy.wait_recv()
    before = jnp.zeros((1, HD), F32)
    own_before = jnp.zeros((1, HD), F32)
    run_rows = []
    for d in range(kv_count):
        shard = run_all[d]
        own_before = jnp.where(me == d, before, own_before)
        run_rows.append(shard + before)
        before = before + shard[R - 1 : R]
    rows_run = jnp.concatenate(run_rows, axis=0)
    M = kv_count * R
    for copy in q_copies:
        copy.wait_recv()
    qp = jnp.concatenate(
        [q_all[:, :, h * HD : (h + 1) * HD].reshape(M, HD) for h in range(H)], axis=0
    )
    row_bias = jnp.concatenate([rows_run[:, h : h + 1] for h in range(H)], axis=0)
    past_bias = jnp.concatenate(
        [jnp.broadcast_to(v_pgate[h : h + 1, :], (M, PL)) for h in range(H)], axis=0
    )
    own_bias = jnp.concatenate(
        [
            jnp.broadcast_to(local_t[h : h + 1, :] + own_before[:, h : h + 1], (M, R))
            for h in range(H)
        ],
        axis=0,
    )
    old = dot_t(qp, v_pk[...]) * scale + past_bias + row_bias
    new = dot_t(qp, key_rows[:R]) * scale + row_bias - own_bias
    causal = me * R + lax.broadcasted_iota(jnp.int32, (M, R), 1) <= lax.broadcasted_iota(
        jnp.int32, (M, R), 0
    )
    causal = jnp.where(causal, 0.0, -jnp.inf)
    new = new + jnp.concatenate([causal] * H, axis=0)
    top = jnp.maximum(jnp.max(old, axis=1, keepdims=True), jnp.max(new, axis=1, keepdims=True))
    old = jnp.exp(old - top)
    new = jnp.exp(new - top)
    total = jnp.sum(old, axis=1, keepdims=True) + jnp.sum(new, axis=1, keepdims=True)
    summed = dot(old.astype(BF16), v_pv[...]) + dot(new.astype(BF16), value_rows[:R])
    lane = lax.broadcasted_iota(jnp.int32, (M, HD), 1)
    stats = jnp.zeros((M, HD), F32)
    for h in range(H):
        part = slice(h * M, (h + 1) * M)
        part_send[:, :, h * HD : (h + 1) * HD] = summed[part].astype(BF16).reshape(kv_count, R, HD)
        stats = jnp.where(lane == h, top[part], stats)
        stats = jnp.where(lane == H + h, total[part], stats)
    stat_send[...] = stats.reshape(kv_count, R, HD)
    part_copies = exchange(lambda peer: part_send.at[peer], part_all, part_ssem, part_rsem)
    stat_copies = exchange(lambda peer: stat_send.at[peer], stat_all, stat_ssem, stat_rsem)
    part_all[me] = part_send[me]
    stat_all[me] = stat_send[me]

    for g in range(early, groups):
        decode_group(g)

    def to_cores(src, dst, ssem, rsem):
        copies = []
        for i in range(1, tp_count):
            copy = pltpu.make_async_remote_copy(
                src_ref=src,
                dst_ref=dst.at[i - 1],
                send_sem=ssem.at[i - 1],
                recv_sem=rsem.at[i - 1],
                device_id={"tp": lax.rem(core + i, tp_count)},
                device_id_type=MESH,
            )
            copy.start()
            copies.append(copy)
        return copies

    ready(v_wo, v_ogain)
    dec_att = jnp.concatenate(
        [att_split[pl.ds(h, N, stride=H), :].astype(BF16) for h in range(H)], axis=1
    )
    dec_part[...] = dot(dec_att, v_wo[...]).astype(BF16)
    tpd_copies = to_cores(dec_part, dec_parts, tpd_ssem, tpd_rsem)

    for copy in stat_copies + part_copies:
        copy.wait_recv()
    stat = [stat_all[d] for d in range(kv_count)]
    best = functools.reduce(jnp.maximum, stat)
    pieces = []
    weights = [jnp.exp(x[:, :H] - best[:, :H]) for x in stat]
    whole = functools.reduce(jnp.add, [x[:, H : 2 * H] * w for x, w in zip(stat, weights)])
    for h in range(H):
        mixed = functools.reduce(
            jnp.add,
            [
                part_all[d, :, h * HD : (h + 1) * HD].astype(F32) * weights[d][:, h : h + 1]
                for d in range(kv_count)
            ],
        )
        pieces.append((mixed / whole[:, h : h + 1]).astype(BF16))
    piece_att = jnp.concatenate(pieces, axis=1)
    piece_part[...] = dot(piece_att, v_wo[...]).astype(BF16)
    tpp_copies = to_cores(piece_part, piece_parts, tpp_ssem, tpp_rsem)

    def finish(part, parts, copies):
        mixed = part[...].astype(F32)
        for i in range(tp_count - 1):
            copies[i].wait_recv()
            mixed = mixed + parts[i].astype(F32)
        return rms_scale(mixed, v_ogain[...])

    final = finish(dec_part, dec_parts, tpd_copies)
    for s in range(S):
        dec_out[s] = final[s * T : (s + 1) * T].astype(BF16)
    piece_out[...] = finish(piece_part, piece_parts, tpp_copies).astype(BF16)
    for copy in q_copies + run_copies + part_copies + stat_copies + tpd_copies + tpp_copies:
        copy.wait_send()


def body(kv_count, tp_count, *args):
    (
        piece_tokens,
        dec_tokens,
        norm_gain,
        query_weight,
        key_weight,
        value_weight,
        gate_weight,
        gate_bias,
        out_weight,
        out_gain,
        past_keys,
        past_values,
        past_gate,
        dec_keys,
        dec_values,
        dec_gate,
        dec_lengths,
    ) = args
    R, D = piece_tokens.shape
    S, T, _ = dec_tokens.shape
    PL, kv_local, HD = past_keys.shape
    DP = dec_keys.shape[1]
    H = gate_bias.shape[0]
    assert kv_local == 1
    N = S * T
    operands = (
        piece_tokens,
        dec_tokens,
        norm_gain.reshape(1, D),
        query_weight,
        key_weight,
        value_weight,
        gate_weight.T,
        gate_bias.reshape(1, H),
        out_weight,
        out_gain.reshape(1, D),
        past_keys.reshape(PL, HD),
        past_values.reshape(PL, HD),
        past_gate,
        dec_keys.reshape(S, DP, HD),
        dec_values.reshape(S, DP, HD),
        dec_gate,
        dec_lengths.reshape(1, S),
    )
    groups = math.gcd(S, 3)
    kv_peers = max(kv_count - 1, 1)
    tp_peers = max(tp_count - 1, 1)
    vmem = pltpu.VMEM
    dma = pltpu.SemaphoreType.DMA
    scratch = [vmem(x.shape, x.dtype) for x in operands] + [
        vmem((R + N, D), F32),
        vmem((N * H, HD), F32),
        vmem((N * H, HD), F32),
        vmem((N * H, HD), F32),
        vmem((R, H * HD), BF16),
        vmem((kv_count, R, H * HD), BF16),
        vmem((R, HD), F32),
        vmem((kv_count, R, HD), F32),
        vmem((kv_count, R, H * HD), BF16),
        vmem((kv_count, R, H * HD), BF16),
        vmem((kv_count, R, HD), F32),
        vmem((kv_count, R, HD), F32),
        vmem((N, D), BF16),
        vmem((tp_peers, N, D), BF16),
        vmem((R, D), BF16),
        vmem((tp_peers, R, D), BF16),
        dma((len(operands),)),
        dma((groups,)),
        dma((groups,)),
    ]
    scratch += [dma((kv_peers,))] * 8 + [dma((tp_peers,))] * 4
    return pl.pallas_call(
        functools.partial(kernel, kv_count, tp_count),
        out_shape=(
            jax.ShapeDtypeStruct((R, D), BF16),
            jax.ShapeDtypeStruct((S, T, D), BF16),
        ),
        in_specs=[pl.BlockSpec(memory_space=pl.ANY)] * len(operands),
        out_specs=(pl.BlockSpec(memory_space=pltpu.VMEM),) * 2,
        scratch_shapes=scratch,
        compiler_params=pltpu.CompilerParams(collective_id=0, has_side_effects=True),
        name="layer",
    )(*operands)


def solution(mesh):
    return jax.shard_map(
        functools.partial(body, mesh.shape["kv"], mesh.shape["tp"]),
        mesh=mesh,
        in_specs=(
            P(("dp", "kv"), None),
            P(("dp", "kv"), None, None),
            P(),
            P(None, "tp"),
            P(None, "tp"),
            P(None, "tp"),
            P(None, "tp"),
            P("tp"),
            P("tp", None),
            P(),
            P(("dp", "kv"), "tp", None),
            P(("dp", "kv"), "tp", None),
            P("tp", ("dp", "kv")),
            P(("dp", "kv"), None, "tp", None),
            P(("dp", "kv"), None, "tp", None),
            P(("dp", "kv"), "tp", None),
            P(("dp", "kv")),
        ),
        out_specs=(P(("dp", "kv"), None), P(("dp", "kv"), None, None)),
        check_vma=False,
    )
```

time: 106 us -> 20.5 us (0.19)
  blocking collectives: 26.8 us -> 0 us
  waiting for transfers between devices: 26.5 us -> 0 us
  Pallas kernels: 0 us -> 16.5 us
  between operations: 14.4 us -> 0.65 us
  matrix products: 12.2 us -> 0 us
  starting transfers between devices: 11.9 us -> 0 us
  other arithmetic: 6.01 us -> 0 us
  local copies, waits for them, and re-layouts: 7.15 us -> 3.16 us
    all_gather x2 -> x0, blocking collectives: 26.8 us -> none  [the longest x1 13.6 us: body(): gathered_run = lax.all_gather(local_run, 'kv', axis=0, tiled=True)]
    psum x1 -> x0, waiting for transfers between devices: 17.4 us -> none  [body(): lax.psum(partial_rows.astype(jnp.bfloat16), 'tp').astype(jnp.float32)]
    pallas_call x0 -> x1, Pallas kernels: none -> 16.5 us  [body(): pl.pallas_call(functools.partial(kernel, kv_count, tp_count), out_shape=(...]
    dot_general x25 -> x0, matrix products: 12.2 us -> none  [the longest x1 2.03 us: body(): jnp.einsum('stkgd,spkd->skgtp', dec_queries, dec_keys, preferred_element_...]
    all_to_all x3 -> x0, starting transfers between devices: 11.9 us -> none  [the longest x1 5.09 us: body(): lax.all_to_all(group_total.reshape(kv_count, piece_rows, heads_local), 'k...]
    all_to_all x3 -> x0, waiting for transfers between devices: 9.01 us -> none  [the longest x1 5.81 us: body(): lax.all_to_all(group_out.reshape(kv_count, piece_rows, heads_local, head_...]
    another operation x10 -> x0, local copies, waits for them, and re-layouts: 3.48 us -> none  [the longest x1 0.85 us: body(): jnp.moveaxis(past_gate.reshape(kv_local, group_size, -1), 1, 0)]
    reduce_sum x14 -> x0, other arithmetic: 3.29 us -> none  [the longest x2 2.09 us: rms_scale(): jnp.mean(widened * widened, axis=-1, keepdims=True) + EPS]
  transfers between devices with their start and end apart: 4 -> 0, of which waited for: 3 -> 0; matrix products, arithmetic and copies ran while one was open for 8% -> 0% of each run, Pallas kernels for 0% -> 0%
where the time goes in v1:
time: 20.5 us; the launch traced here: 20.3 us
  Pallas kernels  16.5 us (80%)
  local copies, waits for them, and re-layouts  3.16 us (15%)
  between operations  0.65 us (3%)
    pallas_call x1, Pallas kernels, body(): pl.pallas_call(functools.partial(kernel, kv_count, tp_count), out_shape=(...  16.5 us
    unnamed x2, local copies, waits for them, and re-layouts  3.16 us

profile of v1, /device:TPU:0, one launch (start us, length us, event | category | flops | bytes accessed | tf_op | source)
XLA Modules:
  0.0 20.3 jit_solution(14775195643349751257)
XLA Ops:
  0.6 16.5 %layer.1 = (bf16[16,2048]{1,0:T(8,128)(2,1)}, bf16[12,4,2048]{2,1,0:T(4,128)(2,1)}) custom-call(bf16[16,2048]{1,0:T(8,128)(2,1)} %piece_tokens.1, bf16[12,4,2048]{2,1,0:T(4,128)(2,1)} %dec_tokens.1, f32[1,2048]{1,0:T(1,128)} %bitcast.14, bf16[2048,512]{1,0:T(8,128)(2,1)} %query_weight.1, bf16[2048,128]{1,0:T(8,128)(2,1)} %key_weight.1, ...), custom_call_target="tpu_custom_call" | custom-call | tf_op jit(solution)/shard_map/layer/pallas_call | solution.py:464
  17.2 1.5 %copy.21 = bf16[16,2048]{1,0:T(8,128)(2,1)} copy(bf16[16,2048]{1,0:T(8,128)(2,1)} %get-tuple-element.4) | data formatting | bytes 131072
  18.7 1.7 %copy.22 = bf16[12,4,2048]{2,1,0:T(4,128)(2,1)} copy(bf16[12,4,2048]{2,1,0:T(4,128)(2,1)} %get-tuple-element.5) | data formatting | bytes 393216

commit v2 on v1

--- a/solution.py
+++ b/solution.py
@@ -87,8 +87,6 @@
     run_all,
     part_send,
     part_all,
-    stat_send,
-    stat_all,
     dec_part,
     dec_parts,
     piece_part,
@@ -102,8 +100,6 @@
     run_rsem,
     part_ssem,
     part_rsem,
-    stat_ssem,
-    stat_rsem,
     tpd_ssem,
     tpd_rsem,
     tpp_ssem,
@@ -127,9 +123,9 @@
         (piece_tokens, v_piece),
         (dec_tokens, v_dec),
         (norm_gain, v_gain),
+        (query_weight, v_wq),
         (gate_weight, v_wg),
         (gate_bias, v_bias),
-        (query_weight, v_wq),
         (key_weight, v_wk),
         (value_weight, v_wv),
         (dec_gate, v_dgate),
@@ -160,9 +156,15 @@
     for src, dst in late:
         start_load(src, dst)
 
-    def ready(*refs):
-        for ref in refs:
-            loads[id(ref)].wait()
+    def ready(name, *refs):
+        with jax.named_scope(name):
+            for ref in refs:
+                loads[id(ref)].wait()
+
+    def arrive(name, copies):
+        with jax.named_scope(name):
+            for copy in copies:
+                copy.wait_recv()
 
     barrier = pltpu.get_barrier_semaphore()
     for i in range(1, kv_count):
@@ -174,48 +176,51 @@
             barrier, inc=1, device_id={"tp": lax.rem(core + i, tp_count)}, device_id_type=MESH
         )
 
-    ready(v_piece, v_dec, v_gain)
+    ready("w_tok", v_piece, v_dec, v_gain)
     rows_x[:R, :] = v_piece[...].astype(F32)
     for s in range(S):
         rows_x[R + s * T : R + (s + 1) * T, :] = v_dec[s].astype(F32)
     normed = rms_scale(rows_x[...], v_gain[...]).astype(BF16)
-    ready(v_wg, v_bias)
+    ready("w_gate", v_wg, v_bias)
     logits = dot_t(normed, v_wg[...]) + v_bias[...]
     log_gates = jnp.minimum(logits, 0.0) - jnp.log1p(jnp.exp(-jnp.abs(logits)))
     log_gates = jnp.concatenate([log_gates, jnp.zeros((R + N, HD - H), F32)], axis=1)
     local_run = running_sum(log_gates[:R], R)
     dec_run = running_sum(log_gates[R:], T)
-    run_send[...] = local_run
-    ready(v_wq)
+    run_send[...] = split_terms(local_run, H).astype(BF16)
+    ready("w_wq", v_wq)
     queries = dot(normed, v_wq[...])
     q_send[...] = queries[:R].astype(BF16)
-    pl.semaphore_wait(barrier, kv_count - 1 + tp_count - 1)
-
-    def exchange(src_of, dst, ssem, rsem):
-        copies = []
-        for i in range(1, kv_count):
-            peer = lax.rem(me + i, kv_count)
-            copy = pltpu.make_async_remote_copy(
-                src_ref=src_of(peer),
-                dst_ref=dst.at[me],
-                send_sem=ssem.at[i - 1],
-                recv_sem=rsem.at[i - 1],
-                device_id={"kv": peer},
-                device_id_type=MESH,
-            )
-            copy.start()
-            copies.append(copy)
-        return copies
-
-    q_copies = exchange(lambda peer: q_send, q_all, q_ssem, q_rsem)
-    run_copies = exchange(lambda peer: run_send, run_all, run_ssem, run_rsem)
+    with jax.named_scope("barrier"):
+        pl.semaphore_wait(barrier, kv_count - 1 + tp_count - 1)
+
+    def send(src, dst, ssem, rsem, i, peer):
+        copy = pltpu.make_async_remote_copy(
+            src_ref=src,
+            dst_ref=dst.at[me],
+            send_sem=ssem.at[i - 1],
+            recv_sem=rsem.at[i - 1],
+            device_id={"kv": peer},
+            device_id_type=MESH,
+        )
+        copy.start()
+        return copy
+
+    places = [partner(me, i, kv_count) for i in range(1, kv_count)]
+    far_first = range(kv_count - 1, 0, -1)
+    run_copies = [
+        send(run_send, run_all, run_ssem, run_rsem, i, places[i - 1]) for i in far_first
+    ]
+    q_copies = [
+        send(q_send, q_all, q_ssem, q_rsem, i, places[i - 1]) for i in far_first
+    ]
     q_all[me] = queries[:R].astype(BF16)
-    run_all[me] = local_run
+    run_all[me] = split_terms(local_run, H).astype(BF16)
 
     for h in range(H):
         q_split[pl.ds(h, N, stride=H), :] = queries[R:, h * HD : (h + 1) * HD]
         run_split[pl.ds(h, N, stride=H), :] = jnp.broadcast_to(dec_run[:, h : h + 1], (N, HD))
-    ready(v_wk, v_wv)
+    ready("w_wkv", v_wk, v_wv)
     key_rows = dot(normed, v_wk[...]).astype(BF16)
     value_rows = dot(normed, v_wv[...]).astype(BF16)
     pad = -(R + N) % 128
@@ -234,13 +239,14 @@
     keep = (row_at >= H * col_at) & (row_at < H * (col_at - col_in + T))
     new_scores = jnp.where(keep, new_scores, -jnp.inf)
 
-    ready(v_dgate, v_len)
+    ready("w_dgate", v_dgate, v_len)
     slot = lax.broadcasted_iota(jnp.int32, (H, DP), 1)
 
     def decode_group(g):
         ck, cv = dec_loads[g]
         lo, hi = g * G * T * H, (g + 1) * G * T * H
-        ck.wait()
+        with jax.named_scope("w_dk"):
+            ck.wait()
         biases, scores = [], []
         for s in range(g * G, (g + 1) * G):
             length = v_len[:, s : s + 1]
@@ -259,7 +265,8 @@
         new = jnp.exp(new - top)
         total = jnp.sum(old, axis=1, keepdims=True) + jnp.sum(new, axis=1, keepdims=True)
         old = old.astype(BF16)
-        cv.wait()
+        with jax.named_scope("w_dv"):
+            cv.wait()
         summed = jnp.concatenate(
             [
                 dot(old[i * T * H : (i + 1) * T * H], v_dv[g * G + i])
@@ -270,66 +277,59 @@
         summed = summed + dot(new.astype(BF16), value_rows[R:])
         att_split[lo:hi, :] = summed / total
 
-    early = max(groups - 1, 1)
-    for g in range(early):
+    for g in range(groups):
         decode_group(g)
 
-    ready(v_pgate, v_pk, v_pv)
-    for copy in run_copies:
-        copy.wait_recv()
+    M = kv_count * R
+    ready("w_past", v_pgate, v_pk, v_pv)
+    past_bias = jnp.concatenate(
+        [jnp.broadcast_to(v_pgate[h : h + 1, :], (M, PL)) for h in range(H)], axis=0
+    )
+    col_place = me * R + lax.broadcasted_iota(jnp.int32, (M, R), 1)
+    row_place = lax.broadcasted_iota(jnp.int32, (M, R), 0)
+    causal = jnp.where(col_place <= row_place, 0.0, -jnp.inf)
+    lane = lax.broadcasted_iota(jnp.int32, (M, HD), 1)
+    arrive("r_run", run_copies)
     before = jnp.zeros((1, HD), F32)
     own_before = jnp.zeros((1, HD), F32)
     run_rows = []
     for d in range(kv_count):
-        shard = run_all[d]
+        shard = join_terms(run_all[d].astype(F32), H)
         own_before = jnp.where(me == d, before, own_before)
         run_rows.append(shard + before)
         before = before + shard[R - 1 : R]
     rows_run = jnp.concatenate(run_rows, axis=0)
-    M = kv_count * R
-    for copy in q_copies:
-        copy.wait_recv()
-    qp = jnp.concatenate(
-        [q_all[:, :, h * HD : (h + 1) * HD].reshape(M, HD) for h in range(H)], axis=0
-    )
     row_bias = jnp.concatenate([rows_run[:, h : h + 1] for h in range(H)], axis=0)
-    past_bias = jnp.concatenate(
-        [jnp.broadcast_to(v_pgate[h : h + 1, :], (M, PL)) for h in range(H)], axis=0
-    )
     own_bias = jnp.concatenate(
         [
-            jnp.broadcast_to(local_t[h : h + 1, :] + own_before[:, h : h + 1], (M, R))
+            causal - (local_t[h : h + 1, :] + own_before[:, h : h + 1])
             for h in range(H)
         ],
         axis=0,
     )
+    arrive("r_q", q_copies)
+    qp = jnp.concatenate(
+        [q_all[:, :, h * HD : (h + 1) * HD].reshape(M, HD) for h in range(H)], axis=0
+    )
     old = dot_t(qp, v_pk[...]) * scale + past_bias + row_bias
-    new = dot_t(qp, key_rows[:R]) * scale + row_bias - own_bias
-    causal = me * R + lax.broadcasted_iota(jnp.int32, (M, R), 1) <= lax.broadcasted_iota(
-        jnp.int32, (M, R), 0
-    )
-    causal = jnp.where(causal, 0.0, -jnp.inf)
-    new = new + jnp.concatenate([causal] * H, axis=0)
+    new = dot_t(qp, key_rows[:R]) * scale + row_bias + own_bias
     top = jnp.maximum(jnp.max(old, axis=1, keepdims=True), jnp.max(new, axis=1, keepdims=True))
     old = jnp.exp(old - top)
     new = jnp.exp(new - top)
     total = jnp.sum(old, axis=1, keepdims=True) + jnp.sum(new, axis=1, keepdims=True)
     summed = dot(old.astype(BF16), v_pv[...]) + dot(new.astype(BF16), value_rows[:R])
-    lane = lax.broadcasted_iota(jnp.int32, (M, HD), 1)
     stats = jnp.zeros((M, HD), F32)
     for h in range(H):
         part = slice(h * M, (h + 1) * M)
         part_send[:, :, h * HD : (h + 1) * HD] = summed[part].astype(BF16).reshape(kv_count, R, HD)
         stats = jnp.where(lane == h, top[part], stats)
         stats = jnp.where(lane == H + h, total[part], stats)
-    stat_send[...] = stats.reshape(kv_count, R, HD)
-    part_copies = exchange(lambda peer: part_send.at[peer], part_all, part_ssem, part_rsem)
-    stat_copies = exchange(lambda peer: stat_send.at[peer], stat_all, stat_ssem, stat_rsem)
+    part_send[:, :, H * HD :] = split_terms(stats, 2 * H).astype(BF16).reshape(kv_count, R, HD)
+    part_copies = [
+        send(part_send.at[places[i - 1]], part_all, part_ssem, part_rsem, i, places[i - 1])
+        for i in far_first
+    ]
     part_all[me] = part_send[me]
-    stat_all[me] = stat_send[me]
-
-    for g in range(early, groups):
-        decode_group(g)
 
     def to_cores(src, dst, ssem, rsem):
         copies = []
@@ -346,16 +346,26 @@
             copies.append(copy)
         return copies
 
-    ready(v_wo, v_ogain)
+    def finish(name, part, parts, copies):
+        mixed = part[...].astype(F32)
+        arrive(name, copies)
+        for i in range(tp_count - 1):
+            mixed = mixed + parts[i].astype(F32)
+        return rms_scale(mixed, v_ogain[...])
+
+    ready("w_wo", v_wo, v_ogain)
     dec_att = jnp.concatenate(
         [att_split[pl.ds(h, N, stride=H), :].astype(BF16) for h in range(H)], axis=1
     )
     dec_part[...] = dot(dec_att, v_wo[...]).astype(BF16)
     tpd_copies = to_cores(dec_part, dec_parts, tpd_ssem, tpd_rsem)
 
-    for copy in stat_copies + part_copies:
-        copy.wait_recv()
-    stat = [stat_all[d] for d in range(kv_count)]
+    final = finish("r_tpd", dec_part, dec_parts, tpd_copies)
+    for s in range(S):
+        dec_out[s] = final[s * T : (s + 1) * T].astype(BF16)
+
+    arrive("r_part", part_copies)
+    stat = [join_terms(part_all[d, :, H * HD :].astype(F32), 2 * H) for d in range(kv_count)]
     best = functools.reduce(jnp.maximum, stat)
     pieces = []
     weights = [jnp.exp(x[:, :H] - best[:, :H]) for x in stat]
@@ -373,19 +383,43 @@
     piece_part[...] = dot(piece_att, v_wo[...]).astype(BF16)
     tpp_copies = to_cores(piece_part, piece_parts, tpp_ssem, tpp_rsem)
 
-    def finish(part, parts, copies):
-        mixed = part[...].astype(F32)
-        for i in range(tp_count - 1):
-            copies[i].wait_recv()
-            mixed = mixed + parts[i].astype(F32)
-        return rms_scale(mixed, v_ogain[...])
-
-    final = finish(dec_part, dec_parts, tpd_copies)
-    for s in range(S):
-        dec_out[s] = final[s * T : (s + 1) * T].astype(BF16)
-    piece_out[...] = finish(piece_part, piece_parts, tpp_copies).astype(BF16)
-    for copy in q_copies + run_copies + part_copies + stat_copies + tpd_copies + tpp_copies:
-        copy.wait_send()
+    piece_out[...] = finish("r_tpp", piece_part, piece_parts, tpp_copies).astype(BF16)
+    with jax.named_scope("sends"):
+        for copy in q_copies + run_copies + part_copies + tpd_copies + tpp_copies:
+            copy.wait_send()
+
+
+def partner(me, i, count):
+    if count & (count - 1):
+        return (me + i) % count
+    other, bit = 0, 1
+    while bit < count:
+        other = other + bit * ((me // bit + i // bit) % 2)
+        bit *= 2
+    return other
+
+
+def split_terms(x, step):
+    high = x.astype(BF16).astype(F32)
+    middle = (x - high).astype(BF16).astype(F32)
+    low = x - high - middle
+    return high + pltpu.roll(middle, step, 1) + pltpu.roll(low, 2 * step, 1)
+
+
+def join_terms(x, step):
+    lanes = x.shape[1]
+    return x + pltpu.roll(x, lanes - step, 1) + pltpu.roll(x, lanes - 2 * step, 1)
+
+
+def write_out(piece, dec, piece_out, dec_out, sems):
+    copies = [
+        pltpu.make_async_copy(dec, dec_out, sems.at[0]),
+        pltpu.make_async_copy(piece, piece_out, sems.at[1]),
+    ]
+    for copy in copies:
+        copy.start()
+    for copy in copies:
+        copy.wait()
 
 
 def body(kv_count, tp_count, *args):
@@ -446,12 +480,10 @@
         vmem((N * H, HD), F32),
         vmem((R, H * HD), BF16),
         vmem((kv_count, R, H * HD), BF16),
-        vmem((R, HD), F32),
-        vmem((kv_count, R, HD), F32),
-        vmem((kv_count, R, H * HD), BF16),
-        vmem((kv_count, R, H * HD), BF16),
-        vmem((kv_count, R, HD), F32),
-        vmem((kv_count, R, HD), F32),
+        vmem((R, HD), BF16),
+        vmem((kv_count, R, HD), BF16),
+        vmem((kv_count, R, (H + 1) * HD), BF16),
+        vmem((kv_count, R, (H + 1) * HD), BF16),
         vmem((N, D), BF16),
         vmem((tp_peers, N, D), BF16),
         vmem((R, D), BF16),
@@ -460,19 +492,27 @@
         dma((groups,)),
         dma((groups,)),
     ]
-    scratch += [dma((kv_peers,))] * 8 + [dma((tp_peers,))] * 4
-    return pl.pallas_call(
+    scratch += [dma((kv_peers,))] * 6 + [dma((tp_peers,))] * 4
+    results = pl.pallas_call(
         functools.partial(kernel, kv_count, tp_count),
-        out_shape=(
-            jax.ShapeDtypeStruct((R, D), BF16),
-            jax.ShapeDtypeStruct((S, T, D), BF16),
-        ),
-        in_specs=[pl.BlockSpec(memory_space=pl.ANY)] * len(operands),
+        out_shape=(vmem((R, D), BF16), vmem((S, T, D), BF16)),
+        in_specs=[pl.BlockSpec(memory_space=pltpu.HBM)] * len(operands),
         out_specs=(pl.BlockSpec(memory_space=pltpu.VMEM),) * 2,
         scratch_shapes=scratch,
         compiler_params=pltpu.CompilerParams(collective_id=0, has_side_effects=True),
         name="layer",
     )(*operands)
+    return pl.pallas_call(
+        write_out,
+        out_shape=(
+            jax.ShapeDtypeStruct((R, D), BF16),
+            jax.ShapeDtypeStruct((S, T, D), BF16),
+        ),
+        in_specs=[pl.BlockSpec(memory_space=vmem)] * 2,
+        out_specs=(pl.BlockSpec(memory_space=pltpu.HBM),) * 2,
+        scratch_shapes=[dma((2,))],
+        name="write_out",
+    )(*[pltpu.with_memory_space_constraint(x, vmem) for x in results])
 
 
 def solution(mesh):

time: 20.5 us -> 16.5 us (0.80)
  local copies, waits for them, and re-layouts: 3.16 us -> 0 us
  Pallas kernels: 16.5 us -> 15.7 us
    unnamed x2 -> x0, local copies, waits for them, and re-layouts: 3.16 us -> none
    pallas_call x1, Pallas kernels: 16.5 us -> 15 us  [body(): pl.pallas_call(functools.partial(kernel, kv_count, tp_count), out_shape=(...]
    pallas_call x0 -> x1, Pallas kernels: none -> 0.71 us  [body(): pl.pallas_call(write_out, out_shape=(jax.ShapeDtypeStruct((R, D), BF16),...]
where the time goes in v2:
time: 16.5 us; the launch traced here: 16.3 us
  Pallas kernels  15.7 us (95%)
  between operations  0.65 us (4%)
    pallas_call x1, Pallas kernels, body(): pl.pallas_call(functools.partial(kernel, kv_count, tp_count), out_shape=(...  15 us
    pallas_call x1, Pallas kernels, body(): pl.pallas_call(write_out, out_shape=(jax.ShapeDtypeStruct((R, D), BF16),...  0.71 us

profile of v2, /device:TPU:0, one launch (start us, length us, event | category | flops | bytes accessed | tf_op | source)
XLA Modules:
  0.0 16.3 jit_solution(9388969696827289872)
XLA Ops:
  0.6 15.0 %layer.1 = (bf16[16,2048]{1,0:T(8,128)(2,1)S(1)}, bf16[12,4,2048]{2,1,0:T(4,128)(2,1)S(1)}) custom-call(bf16[16,2048]{1,0:T(8,128)(2,1)} %piece_tokens.1, bf16[12,4,2048]{2,1,0:T(4,128)(2,1)} %dec_tokens.1, f32[1,2048]{1,0:T(1,128)} %bitcast.14, bf16[2048,512]{1,0:T(8,128)(2,1)} %query_weight.1, bf16[2048,128]{1,0:T(8,128)(2,1)} %key_weight.1, ...), custom_call_target="tpu_custom_call" | custom-call | tf_op jit(solution)/shard_map/layer/pallas_call | solution.py:496
  15.6 0.7 %write_out.1 = (bf16[16,2048]{1,0:T(8,128)(2,1)}, bf16[12,4,2048]{2,1,0:T(4,128)(2,1)}) custom-call(bf16[16,2048]{1,0:T(8,128)(2,1)S(1)} %get-tuple-element.4.piece, bf16[12,4,2048]{2,1,0:T(4,128)(2,1)S(1)} %get-tuple-element.5.dec), custom_call_target="tpu_custom_call" | custom-call | tf_op jit(solution)/shard_map/write_out/pallas_call | solution.py:505
